TPU v7x, 32 devices: a whole 2x2x4 slice. The times are simulated.
32 devices in a mesh: grp: 2 (over x), ep: 16 (over z, y, core).
Axes of the slice: x: 2, y: 2, z: 4, core: 2. Of those that a mesh axis runs over, the one named last changes fastest.
Arguments:
- resid: bfloat16 [384, 2048], P(('grp', 'ep')), parts along dimension 0, may hold values from -6 to 6
- norm_gains: float32 [4, 2048], replicated, may hold values from 0.1 to 1.9
- w_query: bfloat16 [2048, 1024], P(None, 'ep'), may hold values from -0.125 to 0.125
- w_key: bfloat16 [2048, 1024], P(None, 'ep'), may hold values from -0.125 to 0.125
- w_value: bfloat16 [2048, 1024], P(None, 'ep'), may hold values from -0.125 to 0.125
- w_outgate: bfloat16 [2048, 1024], P(None, 'ep'), may hold values from -0.125 to 0.125
- w_igate: bfloat16 [2048, 8], replicated, may hold values from -0.125 to 0.125
- w_fgate: bfloat16 [2048, 8], replicated, may hold values from -0.125 to 0.125
- igate_bias: float32 [8], replicated, may hold values from -1 to 1
- fgate_bias: float32 [8], replicated, may hold values from -1 to 5
- state_matrix: float32 [384, 8, 128, 128], P(('grp', 'ep')), parts along dimension 0, may hold values from -0.8 to 0.8
- state_norm: float32 [384, 8, 128], P(('grp', 'ep')), parts along dimension 0, may hold values from -2.4 to 2.4
- state_max: float32 [384, 8], P(('grp', 'ep')), parts along dimension 0, may hold values from -1 to 1
- w_mix_out: bfloat16 [1024, 2048], replicated, may hold values from -0.1875 to 0.1875
- routes: int32 [384, 2], P(('grp', 'ep')), parts along dimension 0, may hold values from 0 to 15, all different within a row; in each aligned block of 12 rows (0 to 11, 12 to 23, ...) at most 2 rows name the same one
- route_scores: bfloat16 [384, 2], P(('grp', 'ep')), parts along dimension 0, may hold values from 0.099609375 to 1
- expert_gate: bfloat16 [16, 2048, 512], P('ep'), may hold values from -0.125 to 0.125
- expert_up: bfloat16 [16, 2048, 512], P('ep'), may hold values from -0.125 to 0.125
- expert_down: bfloat16 [16, 512, 2048], P('ep'), may hold values from -0.25 to 0.25
- dense_gate: bfloat16 [2048, 8192], P(None, 'ep'), may hold values from -0.125 to 0.125
- dense_up: bfloat16 [2048, 8192], P(None, 'ep'), may hold values from -0.125 to 0.125
- dense_down: bfloat16 [8192, 2048], P('ep'), may hold values from -0.0625 to 0.0625
- branch_weight: bfloat16 [2048], replicated, may hold values from -0.125 to 0.125
Outputs:
- out_stream: bfloat16 [384, 2048], P(('grp', 'ep')), parts along dimension 0
- new_matrix: float32 [384, 8, 128, 128], P(('grp', 'ep')), parts along dimension 0
- new_norm: float32 [384, 8, 128], P(('grp', 'ep')), parts along dimension 0
- new_max: float32 [384, 8], P(('grp', 'ep')), parts along dimension 0
There are 2 independent parts, one for each index of `grp`. A program takes and returns all parts, laid end to end along the dimension named above; an argument that names none is the same for every part. Nothing has to cross between parts.
Inputs may be any that keep to these rules, and one draw needn't show every extreme that they name: `routes`: each row names 2 different experts. In each aligned block of 12 rows (the rows of one device) no expert is named by more than 2 rows, a bound that some block reaches.
All inputs are finite; a program needn't handle non-finite values.
Results may differ from a plain program's by a relative error of at most 0.015.
Values may be sent and summed in bfloat16 or wider, within the bound.
A program may use at most 128 MiB of HBM per device.

v0:
```python
import jax
import jax.numpy as jnp
from jax import lax
from jax.sharding import PartitionSpec as P

CAP = 2


def rms_scale(values, gains):
    return values * lax.rsqrt(jnp.mean(values * values, axis=-1, keepdims=True) + 1e-06) * gains


def expert_batch(picked, gate_matrix, up_matrix, down_matrix):
    gate_out = jnp.einsum("jrd,jdf->jrf", picked, gate_matrix, preferred_element_type=jnp.float32)
    up_out = jnp.einsum("jrd,jdf->jrf", picked, up_matrix, preferred_element_type=jnp.float32)
    hidden = (jax.nn.silu(gate_out) * up_out).astype(jnp.bfloat16)
    return jnp.einsum(
        "jrf,jfd->jrd", hidden, down_matrix, preferred_element_type=jnp.float32
    ).astype(jnp.bfloat16)


def route_tables(routes, route_scores, expert_ids):
    onehot = (routes[:, :, None] == expert_ids[None, None, :]).astype(jnp.float32)
    scores = route_scores.astype(jnp.float32)
    shares = scores / jnp.sum(scores, axis=-1, keepdims=True)
    weights = jnp.sum(shares[:, :, None] * onehot, axis=1)
    hit_count = jnp.sum(onehot, axis=1)
    return (weights, hit_count)


def exchanged_experts(
    branch_in, routes, route_scores, expert_gate, expert_up, expert_down, devices_ep
):
    experts = expert_gate.shape[0] * devices_ep
    weights, hit_count = route_tables(routes, route_scores, jnp.arange(experts, dtype=jnp.int32))
    hit_int = hit_count.astype(jnp.int32)
    rank_index = jnp.cumsum(hit_int, axis=0) - hit_int
    slot_range = jnp.arange(CAP, dtype=jnp.int32)
    chosen = (
        (rank_index.T[:, None, :] == slot_range[None, :, None]) & (hit_count.T[:, None, :] > 0.5)
    ).astype(jnp.float32)
    outgoing = jnp.einsum(
        "ect,td->ecd", chosen.astype(jnp.bfloat16), branch_in, preferred_element_type=jnp.float32
    ).astype(jnp.bfloat16)
    incoming = lax.all_to_all(outgoing, "ep", split_axis=0, concat_axis=1, tiled=True)
    produced = expert_batch(incoming, expert_gate, expert_up, expert_down)
    returned = lax.all_to_all(produced, "ep", split_axis=1, concat_axis=0, tiled=True)
    weighted = chosen * weights.T[:, None, :]
    each_expert = jnp.einsum(
        "ect,ecd->etd", weighted, returned.astype(jnp.float32), precision=lax.Precision.HIGHEST
    )
    return jnp.sum(each_expert.astype(jnp.bfloat16).astype(jnp.float32), axis=0)


def local(
    resid,
    norm_gains,
    w_query,
    w_key,
    w_value,
    w_outgate,
    w_igate,
    w_fgate,
    igate_bias,
    fgate_bias,
    state_matrix,
    state_norm,
    state_max,
    w_mix_out,
    routes,
    route_scores,
    expert_gate,
    expert_up,
    expert_down,
    dense_gate,
    dense_up,
    dense_down,
    branch_weight,
):
    seqs_local = resid.shape[0]
    heads = state_matrix.shape[1]
    head_size = state_matrix.shape[2]
    devices_ep = lax.axis_size("ep")
    resid32 = resid.astype(jnp.float32)
    normed = rms_scale(resid32, norm_gains[0]).astype(jnp.bfloat16)
    row_piece = lax.all_gather(normed, "ep", axis=0, tiled=True)
    projected = jnp.stack(
        [
            jnp.dot(row_piece, matrix, preferred_element_type=jnp.float32).astype(jnp.bfloat16)
            for matrix in (w_query, w_key, w_value, w_outgate)
        ],
        axis=1,
    )
    own_proj = lax.all_to_all(projected, "ep", split_axis=0, concat_axis=2, tiled=True)
    head_shape = (seqs_local, heads, head_size)
    query = own_proj[:, 0].astype(jnp.float32).reshape(head_shape)
    key_heads = own_proj[:, 1].astype(jnp.float32).reshape(head_shape) * head_size ** (-0.5)
    value_heads = own_proj[:, 2].astype(jnp.float32).reshape(head_shape)
    outgate = own_proj[:, 3].astype(jnp.float32).reshape(head_shape)
    ipre = jnp.dot(normed, w_igate, preferred_element_type=jnp.float32) + igate_bias
    fpre = jnp.dot(normed, w_fgate, preferred_element_type=jnp.float32) + fgate_bias
    logf = jax.nn.log_sigmoid(fpre)
    new_max = jnp.maximum(ipre, logf + state_max)
    keep_gain = jnp.exp(logf + state_max - new_max)
    write_gain = jnp.exp(ipre - new_max)
    new_matrix = (
        keep_gain[:, :, None, None] * state_matrix
        + write_gain[:, :, None, None] * value_heads[:, :, :, None] * key_heads[:, :, None, :]
    )
    new_norm = keep_gain[:, :, None] * state_norm + write_gain[:, :, None] * key_heads
    numer = jnp.einsum("shed,shd->she", new_matrix, query, precision=lax.Precision.HIGHEST)
    denom = jnp.sum(new_norm * query, axis=-1)
    cell = numer / jnp.maximum(jnp.abs(denom), 1.0)[:, :, None]
    gated = (
        (jax.nn.sigmoid(outgate) * cell).reshape(seqs_local, heads * head_size).astype(jnp.bfloat16)
    )
    mixed = jnp.dot(gated, w_mix_out, preferred_element_type=jnp.float32)
    middle = resid32 + rms_scale(mixed, norm_gains[1])
    branch_in = rms_scale(middle, norm_gains[2]).astype(jnp.bfloat16)
    all_rows = lax.all_gather(branch_in, "ep", axis=0, tiled=True)
    moe_own = exchanged_experts(
        branch_in, routes, route_scores, expert_gate, expert_up, expert_down, devices_ep
    )
    gate_out = jnp.dot(all_rows, dense_gate, preferred_element_type=jnp.float32)
    up_out = jnp.dot(all_rows, dense_up, preferred_element_type=jnp.float32)
    hidden = (jax.nn.silu(gate_out) * up_out).astype(jnp.bfloat16)
    logit = jnp.dot(all_rows, branch_weight, preferred_element_type=jnp.float32)
    summed = lax.psum_scatter(
        (
            jnp.dot(hidden, dense_down, preferred_element_type=jnp.float32)
            * jax.nn.sigmoid(logit)[:, None]
        ).astype(jnp.bfloat16),
        "ep",
        scatter_dimension=0,
        tiled=True,
    ).astype(jnp.float32)
    combined = moe_own + summed
    out_stream = (middle + rms_scale(combined, norm_gains[3])).astype(jnp.bfloat16)
    return (out_stream, new_matrix, new_norm, new_max)


def solution(mesh):
    placed = (
        P(("grp", "ep"), None),
        P(),
        P(None, "ep"),
        P(None, "ep"),
        P(None, "ep"),
        P(None, "ep"),
        P(),
        P(),
        P(),
        P(),
        P(("grp", "ep"), None, None, None),
        P(("grp", "ep"), None, None),
        P(("grp", "ep"), None),
        P(),
        P(("grp", "ep"), None),
        P(("grp", "ep"), None),
        P("ep", None, None),
        P("ep", None, None),
        P("ep", None, None),
        P(None, "ep"),
        P(None, "ep"),
        P("ep", None),
        P(),
    )
    return jax.shard_map(
        local,
        mesh=mesh,
        in_specs=placed,
        out_specs=(
            P(("grp", "ep"), None),
            P(("grp", "ep"), None, None, None),
            P(("grp", "ep"), None, None),
            P(("grp", "ep"), None),
        ),
        check_vma=False,
    )
```

profile of v0, /device:TPU:17, one launch (start us, length us, event | category | flops | bytes accessed | tf_op | source)
XLA Modules:
  0.0 161.0 jit_solution(14762901746730829710)
XLA Ops:
  0.7 1.0 fusion.62
  1.7 1.0 fusion.30
  2.6 1.0 fusion.61
  3.6 21.5 %all-gather = bf16[16,12,2048]{2,1,0:T(8,128)(2,1)} all-gather(bf16[1,12,2048]{2,1,0:T(8,128)(2,1)S(1)} %fusion.61), channel_id=1, replica_groups=mesh['grp'=2,'ep'=16] {'ep'}, dimensions={0}, use_global_device_ids=true | all-gather | bytes 835584 | tf_op jit(solution)/shard_map/all_gather | solution.py:86
  25.1 1.3 reshape.139
  26.5 0.4 fusion.17
  26.9 0.4 fusion.18
  27.4 0.4 fusion.19
  27.8 0.4 fusion.20
  28.2 0.2 copy.76
  28.4 0.8 reshape.151
  29.2 8.6 %all-to-all-start = ((bf16[16,2,1536]{2,1,0:T(2,128)(2,1)}), bf16[16,2,1536]{2,1,0:T(2,128)(2,1)S(1)}, u32[]{:S(2)}, u32[]{:S(2)}) async-start(bf16[16,2,1536]{2,1,0:T(2,128)(2,1)} %reshape.151), calls=%async_computation | async-start | bytes 196608 | tf_op jit(solution)/shard_map/all_to_all | solution.py:94
  37.8 0.1 copy.85
  37.9 0.1 copy.82
  38.0 0.1 select_reduce_fusion
  38.2 0.2 fusion.54
  38.4 0.2 broadcast_multiply_fusion.2
  38.7 0.1 copy.78
  38.7 0.1 copy.79
  38.8 0.1 copy.81
  39.0 0.1 copy.83
  39.1 0.1 copy.84
  39.2 3.3 %all-to-all-done = bf16[16,2,1536]{2,1,0:T(2,128)(2,1)S(1)} async-done(((bf16[16,2,1536]{2,1,0:T(2,128)(2,1)}), bf16[16,2,1536]{2,1,0:T(2,128)(2,1)S(1)}, u32[]{:S(2)}, u32[]{:S(2)}) %all-to-all-start) | async-done | bytes 98336 | tf_op jit(solution)/shard_map/all_to_all | solution.py:94
  42.5 0.2 reshape.152
  42.7 0.2 all_to_all.32
  42.9 0.2 slice_reduce_fusion
  43.1 0.1 fusion.42
  43.3 0.7 multiply_reduce_fusion.3
  44.0 4.5 %multiply_add_fusion = f32[12,8,128,128]{3,2,1,0:T(8,128)S(1)} fusion(f32[12,8,128,128]{3,2,1,0:T(8,128)} %param.33, f32[12,8,128]{2,1,0:T(8,128)S(1)} %get-tuple-element.14, f32[12,8,128]{2,1,0:T(8,128)S(1)} %get-tuple-element.21, f32[12,8]{1,0:T(8,128)S(1)} %copy.78), kind=kLoop, calls=%fused_computation | loop fusion | flops 4718592 | bytes 12681600 | tf_op jit(solution)/shard_map/add | solution.py:107
  48.5 5.0 %fusion.43 = f32[12,8,1,128]{3,2,1,0:T(1,128)S(1)} fusion(f32[12,8,128,128]{3,2,1,0:T(8,128)S(1)} %multiply_add_fusion, bf16[12,4,1024]{2,1,0:T(4,128)(2,1)S(1)} %all_to_all.32), kind=kOutput, calls=%fused_computation.61 | convolution fusion | flops 18874368 | bytes 6389760 | tf_op jit(solution)/shard_map/shed,shd->she/dot_general | solution.py:111
  53.5 0.1 multiply_convert_fusion.1
  53.6 0.8 multiply_reduce_fusion.2
  54.4 0.2 multiply_reduce_fusion.1
  54.7 0.1 fusion.58
  54.8 22.2 %all-gather.1 = bf16[16,12,2048]{2,1,0:T(8,128)(2,1)} all-gather(bf16[1,12,2048]{2,1,0:T(8,128)(2,1)S(1)} %fusion.58), channel_id=1, replica_groups=mesh['grp'=2,'ep'=16] {'ep'}, dimensions={0}, use_global_device_ids=true | all-gather | bytes 835584 | tf_op jit(solution)/shard_map/all_gather | solution.py:120
  77.0 1.3 reshape.141
  78.3 2.9 %fusion.63 = f32[192,512]{1,0:T(8,128)} fusion(bf16[192,2048]{1,0:T(8,128)(2,1)S(1)} %reshape.141, bf16[2048,512]{1,0:T(8,128)(2,1)} %param.42), kind=kOutput, calls=%fused_computation.106 | convolution fusion | flops 402653184 | bytes 3276800 | tf_op jit(solution)/shard_map/dot_general | solution.py:124
  81.2 0.3 fusion.64
  81.6 0.3 convolution_convert_fusion.2
  81.8 0.8 copy.88
  82.6 6.1 %all-to-all-start.1 = ((bf16[16,2,2048]{2,1,0:T(2,128)(2,1)}), bf16[16,2,2048]{2,1,0:T(2,128)(2,1)S(1)}, u32[]{:S(2)}, u32[]{:S(2)}) async-start(bf16[16,2,2048]{2,1,0:T(2,128)(2,1)} %copy.88), calls=%async_computation.1 | async-start | bytes 262144 | tf_op jit(solution)/shard_map/all_to_all | solution.py:45
  88.7 3.6 %fusion.2 = bf16[192,2048]{1,0:T(8,128)(2,1)} fusion(bf16[512,2048]{1,0:T(8,128)(2,1)S(1)} %copy-done, bf16[192,2048]{1,0:T(8,128)(2,1)S(1)} %reshape.141, bf16[2048,512]{1,0:T(8,128)(2,1)} %param.43, f32[192]{0:T(256)S(1)} %add_divide_fusion, f32[192,512]{1,0:T(8,128)} %fusion.63), kind=kOutput, calls=%fused_computation.4 | convolution fusion | flops 806682624 | bytes 6161152 | tf_op jit(solution)/shard_map/dot_general | solution.py:130
  92.3 1.8 %all-to-all-done.1 = bf16[16,2,2048]{2,1,0:T(2,128)(2,1)S(1)} async-done(((bf16[16,2,2048]{2,1,0:T(2,128)(2,1)}), bf16[16,2,2048]{2,1,0:T(2,128)(2,1)S(1)}, u32[]{:S(2)}, u32[]{:S(2)}) %all-to-all-start.1) | async-done | bytes 131104 | tf_op jit(solution)/shard_map/all_to_all | solution.py:45
  94.2 2.0 %fusion.7 = f32[32,512]{1,0:T(8,128)S(1)} fusion(bf16[32,2048]{1,0:T(8,128)(2,1)S(1)} %reshape.130, bf16[1,2048,512]{2,1,0:T(8,128)(2,1)} %param.39), kind=kOutput, calls=%fused_computation.11 | convolution fusion | flops 67108864 | bytes 2293760 | tf_op jit(solution)/shard_map/jrd,jdf->jrf/dot_general | solution.py:14
  96.2 3.2 %fusion.3 = bf16[1,32,2048]{2,1,0:T(8,128)(2,1)S(1)} fusion(bf16[1,512,2048]{2,1,0:T(8,128)(2,1)} %param.41, bf16[32,2048]{1,0:T(8,128)(2,1)S(1)} %reshape.130, bf16[1,2048,512]{2,1,0:T(8,128)(2,1)} %param.40, f32[32,512]{1,0:T(8,128)S(1)} %fusion.7), kind=kOutput, calls=%fused_computation.7 | convolution fusion | flops 134381568 | bytes 4521984 | tf_op jit(solution)/shard_map/jrf,jfd->jrd/dot_general | solution.py:17
  99.4 0.2 copy.98
  99.7 0.5 broadcast.129
  100.2 1.4 reduce.4
  101.5 0.8 reshape.153
  102.3 6.0 %all-to-all-start.2 = ((bf16[16,2,2048]{2,1,0:T(2,128)(2,1)}), bf16[16,2,2048]{2,1,0:T(2,128)(2,1)S(1)}, u32[]{:S(2)}, u32[]{:S(2)}) async-start(bf16[16,2,2048]{2,1,0:T(2,128)(2,1)} %reshape.153), calls=%async_computation.2 | async-start | bytes 262144 | tf_op jit(solution)/shard_map/all_to_all | solution.py:47
  108.3 28.7 %fusion = bf16[16,2048]{1,0:T(8,128)(2,1)S(1)} fusion(bf16[192,2048]{1,0:T(8,128)(2,1)S(1)} %copy-done.4), kind=kCustom, calls=%all-reduce-scatter | all-reduce-scatter fusion | flops 524289 | bytes 852480
  137.0 2.6 %collective-permute-start = (bf16[16,2048]{1,0:T(8,128)(2,1)S(1)}, bf16[16,2048]{1,0:T(8,128)(2,1)S(1)}, u32[]{:S(2)}, u32[]{:S(2)}) collective-permute-start(bf16[16,2048]{1,0:T(8,128)(2,1)S(1)} %fusion), channel_id=1, source_target_pairs={{0,1},{1,2},{2,3},{3,4},{4,5},{5,6},{6,7},{7,8},{8,9},{9,10},{10,1... | collective-permute-start | bytes 196616
  139.6 5.4 %collective-permute-start.1 = (bf16[16,2048]{1,0:T(8,128)(2,1)S(1)}, bf16[16,2048]{1,0:T(8,128)(2,1)S(1)}, u32[]{:S(2)}, u32[]{:S(2)}) collective-permute-start(bf16[16,2048]{1,0:T(8,128)(2,1)S(1)} %fusion), channel_id=1, source_target_pairs={{0,2},{1,3},{2,4},{3,5},{4,6},{5,7},{6,8},{7,9},{8,10},{9,11},{10,... | collective-permute-start | bytes 196616
  145.0 7.3 %collective-permute-start.2 = (bf16[16,2048]{1,0:T(8,128)(2,1)S(1)}, bf16[16,2048]{1,0:T(8,128)(2,1)S(1)}, u32[]{:S(2)}, u32[]{:S(2)}) collective-permute-start(bf16[16,2048]{1,0:T(8,128)(2,1)S(1)} %fusion), channel_id=1, source_target_pairs={{0,3},{1,4},{2,5},{3,6},{4,7},{5,8},{6,9},{7,10},{8,11},{9,12},{10... | collective-permute-start | bytes 196616
  152.3 1.9 %collective-permute-start.3 = (bf16[12,2048]{1,0:T(8,128)(2,1)S(1)}, bf16[12,2048]{1,0:T(8,128)(2,1)S(1)}, u32[]{:S(2)}, u32[]{:S(2)}) collective-permute-start(bf16[12,2048]{1,0:T(8,128)(2,1)S(1)} %slice.36), channel_id=1, source_target_pairs={{0,4},{1,5},{2,6},{3,7},{4,8},{5,9},{6,10},{7,11},{8,12},{9,13},{1... | collective-permute-start | bytes 147464
  154.3 0.6 dynamic-slice.4
  155.6 1.8 %collective-permute-done.3 = bf16[12,2048]{1,0:T(8,128)(2,1)S(1)} collective-permute-done((bf16[12,2048]{1,0:T(8,128)(2,1)S(1)}, bf16[12,2048]{1,0:T(8,128)(2,1)S(1)}, u32[]{:S(2)}, u32[]{:S(2)}) %collective-permute-start.3) | collective-permute-done | bytes 49184
  157.3 0.7 concatenate
  158.1 0.1 reshape.154
  158.2 0.7 bitcast_reduce_fusion
  159.0 0.1 all_to_all.35
  159.1 1.1 fusion.9
  160.1 0.2 multiply_reduce_fusion
  160.3 0.7 add_convert_fusion
  (67 shorter events, 0.6 us)
Async XLA Ops:
  0.6 88.1 %copy-start = (bf16[512,2048]{1,0:T(8,128)(2,1)S(1)}, bf16[512,2048]{1,0:T(8,128)(2,1)}, u32[]{:S(2)}) copy-start(bf16[512,2048]{1,0:T(8,128)(2,1)} %param.44) | copy-start | bytes 6291460
  0.6 25.8 %copy-start.5 = (bf16[2048,64]{0,1:T(8,128)(2,1)S(1)}, bf16[2048,64]{0,1:T(8,128)(2,1)}, u32[]{:S(2)}) copy-start(bf16[2048,64]{0,1:T(8,128)(2,1)} %param.25) | copy-start | bytes 786436
  2.6 24.2 %copy-start.6 = (bf16[2048,64]{0,1:T(8,128)(2,1)S(1)}, bf16[2048,64]{0,1:T(8,128)(2,1)}, u32[]{:S(2)}) copy-start(bf16[2048,64]{0,1:T(8,128)(2,1)} %param.26) | copy-start | bytes 786436
  26.4 1.0 copy-start.7
  26.4 1.3 copy-start.8
  26.8 10.9 %copy-start.14 = (bf16[12,2]{0,1:T(2,128)(2,1)S(1)}, bf16[12,2]{0,1:T(2,128)(2,1)}, u32[]{:S(2)}) copy-start(bf16[12,2]{0,1:T(2,128)(2,1)} %param.38) | copy-start | bytes 148
  26.9 11.1 %copy-start.12 = (s32[12,2]{0,1:T(2,128)S(1)}, s32[12,2]{0,1:T(2,128)}, u32[]{:S(2)}) copy-start(s32[12,2]{0,1:T(2,128)} %param.37) | copy-start | bytes 292
  26.9 11.3 %copy-start.3 = (bf16[12,2048]{1,0:T(8,128)(2,1)S(1)}, bf16[12,2048]{1,0:T(8,128)(2,1)}, u32[]{:S(2)}) copy-start(bf16[12,2048]{1,0:T(8,128)(2,1)} %param.23) | copy-start | bytes 147460
  26.9 11.3 %copy-start.15 = (bf16[2048,8]{0,1:T(8,128)(2,1)S(1)}, bf16[2048,8]{0,1:T(8,128)(2,1)}, u32[]{:S(2)}) copy-start(bf16[2048,8]{0,1:T(8,128)(2,1)} %param.30) | copy-start | bytes 98308
  26.9 11.3 %copy-start.17 = (f32[12,8]{0,1:T(8,128)S(1)}, f32[12,8]{0,1:T(8,128)}, u32[]{:S(2)}) copy-start(f32[12,8]{0,1:T(8,128)} %param.35) | copy-start | bytes 1156
  26.9 11.3 %copy-start.18 = (f32[8]{0:T(128)S(1)}, f32[8]{0:T(128)}, u32[]{:S(2)}) copy-start(f32[8]{0:T(128)} %param.32) | copy-start | bytes 100
  26.9 11.5 %copy-start.16 = (bf16[2048,8]{0,1:T(8,128)(2,1)S(1)}, bf16[2048,8]{0,1:T(8,128)(2,1)}, u32[]{:S(2)}) copy-start(bf16[2048,8]{0,1:T(8,128)(2,1)} %param.29) | copy-start | bytes 98308
  26.9 11.5 %copy-start.19 = (f32[8]{0:T(128)S(1)}, f32[8]{0:T(128)}, u32[]{:S(2)}) copy-start(f32[8]{0:T(128)} %param.31) | copy-start | bytes 100
  27.4 11.5 %copy-start.10 = (bf16[2048]{0:T(1024)(128)(2,1)S(1)}, bf16[2048]{0:T(1024)(128)(2,1)}, u32[]{:S(2)}) copy-start(bf16[2048]{0:T(1024)(128)(2,1)} %param.45) | copy-start | bytes 12292
  27.8 15.5 %copy-start.9 = (f32[12,8,128]{2,1,0:T(8,128)S(1)}, f32[12,8,128]{2,1,0:T(8,128)}, u32[]{:S(2)}) copy-start(f32[12,8,128]{2,1,0:T(8,128)} %param.34) | copy-start | bytes 147460
  29.2 13.3 %all-to-all-start = ((bf16[16,2,1536]{2,1,0:T(2,128)(2,1)}), bf16[16,2,1536]{2,1,0:T(2,128)(2,1)S(1)}, u32[]{:S(2)}, u32[]{:S(2)}) async-start(bf16[16,2,1536]{2,1,0:T(2,128)(2,1)} %reshape.151), calls=%async_computation | async-start | bytes 196608 | tf_op jit(solution)/shard_map/all_to_all | solution.py:94
  38.6 9.8 %copy-start.11 = (f32[12,8]{0,1:T(8,128)}, f32[12,8]{0,1:T(8,128)S(1)}, u32[]{:S(2)}) copy-start(f32[12,8]{0,1:T(8,128)S(1)} %get-tuple-element.10) | copy-start | bytes 1156
  48.5 5.0 %copy-start.1 = (f32[12,8,128,128]{3,2,1,0:T(8,128)}, f32[12,8,128,128]{3,2,1,0:T(8,128)S(1)}, u32[]{:S(2)}) copy-start(f32[12,8,128,128]{3,2,1,0:T(8,128)S(1)} %multiply_add_fusion) | copy-start | bytes 18874372
  48.5 5.1 %copy-start.2 = (bf16[1024,2048]{1,0:T(8,128)(2,1)S(1)}, bf16[1024,2048]{1,0:T(8,128)(2,1)}, u32[]{:S(2)}) copy-start(bf16[1024,2048]{1,0:T(8,128)(2,1)} %param.36) | copy-start | bytes 12582916
  82.6 11.5 %all-to-all-start.1 = ((bf16[16,2,2048]{2,1,0:T(2,128)(2,1)}), bf16[16,2,2048]{2,1,0:T(2,128)(2,1)S(1)}, u32[]{:S(2)}, u32[]{:S(2)}) async-start(bf16[16,2,2048]{2,1,0:T(2,128)(2,1)} %copy.88), calls=%async_computation.1 | async-start | bytes 262144 | tf_op jit(solution)/shard_map/all_to_all | solution.py:45
  96.2 12.1 %copy-start.4 = (bf16[192,2048]{1,0:T(8,128)(2,1)S(1)}, bf16[192,2048]{1,0:T(8,128)(2,1)}, u32[]{:S(2)}) copy-start(bf16[192,2048]{1,0:T(8,128)(2,1)} %fusion.2) | copy-start | bytes 2359300
  99.4 54.9 %copy-start.13 = (u32[32]{0:T(128)S(1)}, u32[32]{0:T(128)}, u32[]{:S(2)}) copy-start(u32[32]{0:T(128)} %constant.42) | copy-start | bytes 388
  102.3 55.8 %all-to-all-start.2 = ((bf16[16,2,2048]{2,1,0:T(2,128)(2,1)}), bf16[16,2,2048]{2,1,0:T(2,128)(2,1)S(1)}, u32[]{:S(2)}, u32[]{:S(2)}) async-start(bf16[16,2,2048]{2,1,0:T(2,128)(2,1)} %reshape.153), calls=%async_computation.2 | async-start | bytes 262144 | tf_op jit(solution)/shard_map/all_to_all | solution.py:47
  137.0 20.4 %collective-permute-start = (bf16[16,2048]{1,0:T(8,128)(2,1)S(1)}, bf16[16,2048]{1,0:T(8,128)(2,1)S(1)}, u32[]{:S(2)}, u32[]{:S(2)}) collective-permute-start(bf16[16,2048]{1,0:T(8,128)(2,1)S(1)} %fusion), channel_id=1, source_target_pairs={{0,1},{1,2},{2,3},{3,4},{4,5},{5,6},{6,7},{7,8},{8,9},{9,10},{10,1... | collective-permute-start | bytes 196616
  139.6 17.7 %collective-permute-start.1 = (bf16[16,2048]{1,0:T(8,128)(2,1)S(1)}, bf16[16,2048]{1,0:T(8,128)(2,1)S(1)}, u32[]{:S(2)}, u32[]{:S(2)}) collective-permute-start(bf16[16,2048]{1,0:T(8,128)(2,1)S(1)} %fusion), channel_id=1, source_target_pairs={{0,2},{1,3},{2,4},{3,5},{4,6},{5,7},{6,8},{7,9},{8,10},{9,11},{10,... | collective-permute-start | bytes 196616
  145.0 12.3 %collective-permute-start.2 = (bf16[16,2048]{1,0:T(8,128)(2,1)S(1)}, bf16[16,2048]{1,0:T(8,128)(2,1)S(1)}, u32[]{:S(2)}, u32[]{:S(2)}) collective-permute-start(bf16[16,2048]{1,0:T(8,128)(2,1)S(1)} %fusion), channel_id=1, source_target_pairs={{0,3},{1,4},{2,5},{3,6},{4,7},{5,8},{6,9},{7,10},{8,11},{9,12},{10... | collective-permute-start | bytes 196616
  152.3 5.0 %collective-permute-start.3 = (bf16[12,2048]{1,0:T(8,128)(2,1)S(1)}, bf16[12,2048]{1,0:T(8,128)(2,1)S(1)}, u32[]{:S(2)}, u32[]{:S(2)}) collective-permute-start(bf16[12,2048]{1,0:T(8,128)(2,1)S(1)} %slice.36), channel_id=1, source_target_pairs={{0,4},{1,5},{2,6},{3,7},{4,8},{5,9},{6,10},{7,11},{8,12},{9,13},{1... | collective-permute-start | bytes 147464
where the time goes:
time: 162 us; the launch traced here: 161 us
  blocking collectives  72.4 us (45%)
  starting transfers between devices  37.8 us (23%)
  matrix products  21.1 us (13%)
  local copies, waits for them, and re-layouts  10.5 us (6%)
  other arithmetic  10.4 us (6%)
  waiting for transfers between devices  6.9 us (4%)
  between operations  1.84 us (1%)
    unnamed x1, blocking collectives  28.7 us
    all_gather x1, blocking collectives, local(): all_rows = lax.all_gather(branch_in, 'ep', axis=0, tiled=True)  22.2 us
    all_gather x1, blocking collectives, local(): row_piece = lax.all_gather(normed, 'ep', axis=0, tiled=True)  21.5 us
    unnamed x4, starting transfers between devices  17.2 us
    all_to_all x1, starting transfers between devices, local(): lax.all_to_all(projected, 'ep', split_axis=0, concat_axis=2, tiled=True)  8.56 us
    unnamed x55, local copies, waits for them, and re-layouts  6.65 us
    all_to_all x1, starting transfers between devices, exchanged_experts(): lax.all_to_all(outgoing, 'ep', split_axis=0, concat_axis=1, tiled=True)  6.08 us
    all_to_all x1, starting transfers between devices, exchanged_experts(): lax.all_to_all(produced, 'ep', split_axis=1, concat_axis=0, tiled=True)  5.97 us
  transfers between devices with their start and end apart: 7, of which 3 were waited for; matrix products, arithmetic and copies ran while one was open for 22% of the time, Pallas kernels for 0%

commit v1 on v0

--- a/solution.py
+++ b/solution.py
@@ -77,13 +77,19 @@
     dense_down,
     branch_weight,
 ):
+
+    def process_the_inputs(x0, axis_tag):
+        return jnp.concatenate(
+            lax.all_to_all(jnp.stack(lax.axis_size(axis_tag) * [x0], 0), axis_tag, 0, 0), axis=0
+        )
+
     seqs_local = resid.shape[0]
     heads = state_matrix.shape[1]
     head_size = state_matrix.shape[2]
     devices_ep = lax.axis_size("ep")
     resid32 = resid.astype(jnp.float32)
     normed = rms_scale(resid32, norm_gains[0]).astype(jnp.bfloat16)
-    row_piece = lax.all_gather(normed, "ep", axis=0, tiled=True)
+    row_piece = process_the_inputs(normed, "ep")
     projected = jnp.stack(
         [
             jnp.dot(row_piece, matrix, preferred_element_type=jnp.float32).astype(jnp.bfloat16)

time: 162 us -> 169 us (1.043)
  waiting for transfers between devices: 6.9 us -> 31.7 us
  blocking collectives: 72.4 us -> 50.7 us
  starting transfers between devices: 37.8 us -> 41.3 us
    all_to_all x0 -> x1, waiting for transfers between devices: none -> 23.4 us  [process_the_inputs(): lax.all_to_all(jnp.stack(lax.axis_size(axis_tag) * [x0], 0), axis_tag, 0, 0)]
    all_gather x1 -> x0, blocking collectives: 21.5 us -> none  [local(): row_piece = lax.all_gather(normed, 'ep', axis=0, tiled=True)]
    all_to_all x0 -> x1, starting transfers between devices: none -> 6.6 us  [process_the_inputs(): lax.all_to_all(jnp.stack(lax.axis_size(axis_tag) * [x0], 0), axis_tag, 0, 0)]
    all_to_all x1, starting transfers between devices: 8.56 us -> 5.12 us  [local(): lax.all_to_all(projected, 'ep', split_axis=0, concat_axis=2, tiled=True)]
    unnamed x55 -> x54, local copies, waits for them, and re-layouts: 6.65 us -> 5.46 us
  transfers between devices with their start and end apart: 7 -> 8, of which waited for: 3 -> 4; matrix products, arithmetic and copies ran while one was open for 22% -> 21% of each run, Pallas kernels for 0% -> 0%
where the time goes in v1:
time: 169 us
  blocking collectives  50.7 us (30%)
  starting transfers between devices  41.3 us (24%)
  waiting for transfers between devices  31.7 us (19%)
  matrix products  21 us (12%)
  local copies, waits for them, and re-layouts  11.7 us (7%)
  other arithmetic  10.4 us (6%)
  between operations  1.82 us (1%)
    unnamed x1, blocking collectives  28.7 us
    all_to_all x1, waiting for transfers between devices, process_the_inputs(): lax.all_to_all(jnp.stack(lax.axis_size(axis_tag) * [x0], 0), axis_tag, 0, 0)  23.4 us
    all_gather x1, blocking collectives, local(): all_rows = lax.all_gather(branch_in, 'ep', axis=0, tiled=True)  22 us
    unnamed x4, starting transfers between devices  17.2 us
    all_to_all x1, starting transfers between devices, process_the_inputs(): lax.all_to_all(jnp.stack(lax.axis_size(axis_tag) * [x0], 0), axis_tag, 0, 0)  6.6 us
    all_to_all x1, starting transfers between devices, exchanged_experts(): lax.all_to_all(outgoing, 'ep', split_axis=0, concat_axis=1, tiled=True)  6.38 us
    all_to_all x1, starting transfers between devices, exchanged_experts(): lax.all_to_all(produced, 'ep', split_axis=1, concat_axis=0, tiled=True)  5.97 us
    unnamed x54, local copies, waits for them, and re-layouts  5.46 us
  transfers between devices with their start and end apart: 8, of which 4 were waited for; matrix products, arithmetic and copies ran while one was open for 21% of the time, Pallas kernels for 0%

profile of v1, /device:TPU:17, one launch (start us, length us, event | category | flops | bytes accessed | tf_op | source)
XLA Modules:
  0.0 168.6 jit_solution(10048920712850791843)
XLA Ops:
  0.7 1.0 fusion.59
  1.7 1.0 fusion.30
  2.7 0.9 fusion.32
  3.6 1.1 stack.12
  4.7 6.6 %all-to-all-start = ((bf16[16,12,2048]{2,1,0:T(8,128)(2,1)}), bf16[16,12,2048]{2,1,0:T(8,128)(2,1)}, u32[]{:S(2)}, u32[]{:S(2)}) async-start(bf16[16,12,2048]{2,1,0:T(8,128)(2,1)} %stack.12), calls=%async_computation | async-start | bytes 2097152 | tf_op jit(solution)/shard_map/all_to_all | solution.py:83
  11.3 0.1 fusion.54
  11.5 0.1 broadcast_multiply_fusion.2
  12.0 0.1 copy.85
  12.1 0.1 copy.82
  12.2 0.1 select_reduce_fusion
  12.4 0.1 copy.83
  12.4 0.1 copy.84
  12.5 23.4 %all-to-all-done = bf16[16,12,2048]{2,1,0:T(8,128)(2,1)} async-done(((bf16[16,12,2048]{2,1,0:T(8,128)(2,1)}), bf16[16,12,2048]{2,1,0:T(8,128)(2,1)}, u32[]{:S(2)}, u32[]{:S(2)}) %all-to-all-start) | async-done | bytes 786464 | tf_op jit(solution)/shard_map/all_to_all | solution.py:83
  36.0 1.3 reshape.134
  37.3 0.4 fusion.17
  37.7 0.4 fusion.18
  38.1 0.2 copy-done.7
  38.3 0.4 fusion.19
  38.7 0.4 fusion.20
  39.1 0.2 copy.76
  39.3 0.8 reshape.155
  40.1 5.1 %all-to-all-start.1 = ((bf16[16,2,1536]{2,1,0:T(2,128)(2,1)}), bf16[16,2,1536]{2,1,0:T(2,128)(2,1)S(1)}, u32[]{:S(2)}, u32[]{:S(2)}) async-start(bf16[16,2,1536]{2,1,0:T(2,128)(2,1)} %reshape.155), calls=%async_computation.1 | async-start | bytes 196608 | tf_op jit(solution)/shard_map/all_to_all | solution.py:100
  45.2 4.7 %all-to-all-done.1 = bf16[16,2,1536]{2,1,0:T(2,128)(2,1)S(1)} async-done(((bf16[16,2,1536]{2,1,0:T(2,128)(2,1)}), bf16[16,2,1536]{2,1,0:T(2,128)(2,1)S(1)}, u32[]{:S(2)}, u32[]{:S(2)}) %all-to-all-start.1) | async-done | bytes 98336 | tf_op jit(solution)/shard_map/all_to_all | solution.py:100
  49.9 0.2 reshape.156
  50.2 0.2 all_to_all.36
  50.3 0.2 slice_reduce_fusion
  50.5 0.1 fusion.42
  50.7 0.7 multiply_reduce_fusion.3
  51.4 4.5 %multiply_add_fusion = f32[12,8,128,128]{3,2,1,0:T(8,128)S(1)} fusion(f32[12,8,128,128]{3,2,1,0:T(8,128)} %param.33, f32[12,8,128]{2,1,0:T(8,128)S(1)} %get-tuple-element.14, f32[12,8,128]{2,1,0:T(8,128)S(1)} %get-tuple-element.21, f32[12,8]{1,0:T(8,128)S(1)} %copy.78), kind=kLoop, calls=%fused_computation | loop fusion | flops 4718592 | bytes 12681600 | tf_op jit(solution)/shard_map/add | solution.py:113
  55.9 5.0 %fusion.43 = f32[12,8,1,128]{3,2,1,0:T(1,128)S(1)} fusion(f32[12,8,128,128]{3,2,1,0:T(8,128)S(1)} %multiply_add_fusion, bf16[12,4,1024]{2,1,0:T(4,128)(2,1)S(1)} %all_to_all.36), kind=kOutput, calls=%fused_computation.61 | convolution fusion | flops 18874368 | bytes 6389760 | tf_op jit(solution)/shard_map/shed,shd->she/dot_general | solution.py:117
  60.9 0.1 multiply_convert_fusion.1
  61.1 0.8 multiply_reduce_fusion.2
  61.9 0.2 multiply_reduce_fusion.1
  62.1 0.1 fusion.58
  62.2 22.0 %all-gather = bf16[16,12,2048]{2,1,0:T(8,128)(2,1)} all-gather(bf16[1,12,2048]{2,1,0:T(8,128)(2,1)S(1)} %fusion.58), channel_id=1, replica_groups=mesh['grp'=2,'ep'=16] {'ep'}, dimensions={0}, use_global_device_ids=true | all-gather | bytes 835584 | tf_op jit(solution)/shard_map/all_gather | solution.py:126
  84.3 1.3 reshape.145
  85.6 2.9 %fusion.60 = f32[192,512]{1,0:T(8,128)} fusion(bf16[192,2048]{1,0:T(8,128)(2,1)S(1)} %reshape.145, bf16[2048,512]{1,0:T(8,128)(2,1)} %param.42), kind=kOutput, calls=%fused_computation.105 | convolution fusion | flops 402653184 | bytes 3276800 | tf_op jit(solution)/shard_map/dot_general | solution.py:130
  88.5 0.3 fusion.61
  88.8 0.3 convolution_convert_fusion.2
  89.1 0.8 copy.88
  89.9 6.4 %all-to-all-start.2 = ((bf16[16,2,2048]{2,1,0:T(2,128)(2,1)}), bf16[16,2,2048]{2,1,0:T(2,128)(2,1)S(1)}, u32[]{:S(2)}, u32[]{:S(2)}) async-start(bf16[16,2,2048]{2,1,0:T(2,128)(2,1)} %copy.88), calls=%async_computation.2 | async-start | bytes 262144 | tf_op jit(solution)/shard_map/all_to_all | solution.py:45
  96.2 3.6 %fusion.2 = bf16[192,2048]{1,0:T(8,128)(2,1)} fusion(bf16[512,2048]{1,0:T(8,128)(2,1)S(1)} %copy-done, bf16[192,2048]{1,0:T(8,128)(2,1)S(1)} %reshape.145, bf16[2048,512]{1,0:T(8,128)(2,1)} %param.43, f32[192]{0:T(256)S(1)} %add_divide_fusion, f32[192,512]{1,0:T(8,128)} %fusion.60), kind=kOutput, calls=%fused_computation.4 | convolution fusion | flops 806682624 | bytes 6161152 | tf_op jit(solution)/shard_map/dot_general | solution.py:136
  99.9 1.8 %all-to-all-done.2 = bf16[16,2,2048]{2,1,0:T(2,128)(2,1)S(1)} async-done(((bf16[16,2,2048]{2,1,0:T(2,128)(2,1)}), bf16[16,2,2048]{2,1,0:T(2,128)(2,1)S(1)}, u32[]{:S(2)}, u32[]{:S(2)}) %all-to-all-start.2) | async-done | bytes 131104 | tf_op jit(solution)/shard_map/all_to_all | solution.py:45
  101.7 2.0 %fusion.7 = f32[32,512]{1,0:T(8,128)S(1)} fusion(bf16[32,2048]{1,0:T(8,128)(2,1)S(1)} %reshape.136, bf16[1,2048,512]{2,1,0:T(8,128)(2,1)} %param.39), kind=kOutput, calls=%fused_computation.11 | convolution fusion | flops 67108864 | bytes 2293760 | tf_op jit(solution)/shard_map/jrd,jdf->jrf/dot_general | solution.py:14
  103.8 3.2 %fusion.3 = bf16[1,32,2048]{2,1,0:T(8,128)(2,1)S(1)} fusion(bf16[1,512,2048]{2,1,0:T(8,128)(2,1)} %param.41, bf16[32,2048]{1,0:T(8,128)(2,1)S(1)} %reshape.136, bf16[1,2048,512]{2,1,0:T(8,128)(2,1)} %param.40, f32[32,512]{1,0:T(8,128)S(1)} %fusion.7), kind=kOutput, calls=%fused_computation.7 | convolution fusion | flops 134381568 | bytes 4521984 | tf_op jit(solution)/shard_map/jrf,jfd->jrd/dot_general | solution.py:17
  107.0 0.2 copy.98
  107.2 0.5 broadcast.131
  107.7 1.4 reduce.4
  109.1 0.8 reshape.157
  109.8 6.0 %all-to-all-start.3 = ((bf16[16,2,2048]{2,1,0:T(2,128)(2,1)}), bf16[16,2,2048]{2,1,0:T(2,128)(2,1)S(1)}, u32[]{:S(2)}, u32[]{:S(2)}) async-start(bf16[16,2,2048]{2,1,0:T(2,128)(2,1)} %reshape.157), calls=%async_computation.3 | async-start | bytes 262144 | tf_op jit(solution)/shard_map/all_to_all | solution.py:47
  115.8 28.7 %fusion = bf16[16,2048]{1,0:T(8,128)(2,1)S(1)} fusion(bf16[192,2048]{1,0:T(8,128)(2,1)S(1)} %copy-done.4), kind=kCustom, calls=%all-reduce-scatter | all-reduce-scatter fusion | flops 524289 | bytes 852480
  144.5 2.6 %collective-permute-start = (bf16[16,2048]{1,0:T(8,128)(2,1)S(1)}, bf16[16,2048]{1,0:T(8,128)(2,1)S(1)}, u32[]{:S(2)}, u32[]{:S(2)}) collective-permute-start(bf16[16,2048]{1,0:T(8,128)(2,1)S(1)} %fusion), channel_id=1, source_target_pairs={{0,1},{1,2},{2,3},{3,4},{4,5},{5,6},{6,7},{7,8},{8,9},{9,10},{10,1... | collective-permute-start | bytes 196616
  147.2 5.4 %collective-permute-start.1 = (bf16[16,2048]{1,0:T(8,128)(2,1)S(1)}, bf16[16,2048]{1,0:T(8,128)(2,1)S(1)}, u32[]{:S(2)}, u32[]{:S(2)}) collective-permute-start(bf16[16,2048]{1,0:T(8,128)(2,1)S(1)} %fusion), channel_id=1, source_target_pairs={{0,2},{1,3},{2,4},{3,5},{4,6},{5,7},{6,8},{7,9},{8,10},{9,11},{10,... | collective-permute-start | bytes 196616
  152.6 7.3 %collective-permute-start.2 = (bf16[16,2048]{1,0:T(8,128)(2,1)S(1)}, bf16[16,2048]{1,0:T(8,128)(2,1)S(1)}, u32[]{:S(2)}, u32[]{:S(2)}) collective-permute-start(bf16[16,2048]{1,0:T(8,128)(2,1)S(1)} %fusion), channel_id=1, source_target_pairs={{0,3},{1,4},{2,5},{3,6},{4,7},{5,8},{6,9},{7,10},{8,11},{9,12},{10... | collective-permute-start | bytes 196616
  159.9 1.9 %collective-permute-start.3 = (bf16[12,2048]{1,0:T(8,128)(2,1)S(1)}, bf16[12,2048]{1,0:T(8,128)(2,1)S(1)}, u32[]{:S(2)}, u32[]{:S(2)}) collective-permute-start(bf16[12,2048]{1,0:T(8,128)(2,1)S(1)} %slice.36), channel_id=1, source_target_pairs={{0,4},{1,5},{2,6},{3,7},{4,8},{5,9},{6,10},{7,11},{8,12},{9,13},{1... | collective-permute-start | bytes 147464
  161.9 0.6 dynamic-slice.4
  163.1 1.8 %collective-permute-done.3 = bf16[12,2048]{1,0:T(8,128)(2,1)S(1)} collective-permute-done((bf16[12,2048]{1,0:T(8,128)(2,1)S(1)}, bf16[12,2048]{1,0:T(8,128)(2,1)S(1)}, u32[]{:S(2)}, u32[]{:S(2)}) %collective-permute-start.3) | collective-permute-done | bytes 49184
  164.9 0.7 concatenate
  165.7 0.1 reshape.158
  165.8 0.7 bitcast_reduce_fusion
  166.5 0.1 all_to_all.39
  166.6 1.1 fusion.9
  167.7 0.2 multiply_reduce_fusion
  167.8 0.7 add_convert_fusion
  (69 shorter events, 0.8 us)
Async XLA Ops:
  0.6 95.6 %copy-start = (bf16[512,2048]{1,0:T(8,128)(2,1)S(1)}, bf16[512,2048]{1,0:T(8,128)(2,1)}, u32[]{:S(2)}) copy-start(bf16[512,2048]{1,0:T(8,128)(2,1)} %param.44) | copy-start | bytes 6291460
  0.7 10.7 %copy-start.15 = (bf16[2048,8]{0,1:T(8,128)(2,1)S(1)}, bf16[2048,8]{0,1:T(8,128)(2,1)}, u32[]{:S(2)}) copy-start(bf16[2048,8]{0,1:T(8,128)(2,1)} %param.30) | copy-start | bytes 98308
  0.7 10.7 %copy-start.18 = (f32[8]{0:T(128)S(1)}, f32[8]{0:T(128)}, u32[]{:S(2)}) copy-start(f32[8]{0:T(128)} %param.32) | copy-start | bytes 100
  0.7 10.7 %copy-start.17 = (f32[12,8]{0,1:T(8,128)S(1)}, f32[12,8]{0,1:T(8,128)}, u32[]{:S(2)}) copy-start(f32[12,8]{0,1:T(8,128)} %param.35) | copy-start | bytes 1156
  0.7 10.8 %copy-start.16 = (bf16[2048,8]{0,1:T(8,128)(2,1)S(1)}, bf16[2048,8]{0,1:T(8,128)(2,1)}, u32[]{:S(2)}) copy-start(bf16[2048,8]{0,1:T(8,128)(2,1)} %param.29) | copy-start | bytes 98308
  0.7 10.8 %copy-start.19 = (f32[8]{0:T(128)S(1)}, f32[8]{0:T(128)}, u32[]{:S(2)}) copy-start(f32[8]{0:T(128)} %param.31) | copy-start | bytes 100
  0.7 11.2 %copy-start.10 = (bf16[2048]{0:T(1024)(128)(2,1)S(1)}, bf16[2048]{0:T(1024)(128)(2,1)}, u32[]{:S(2)}) copy-start(bf16[2048]{0:T(1024)(128)(2,1)} %param.45) | copy-start | bytes 12292
  0.7 11.2 %copy-start.14 = (bf16[12,2]{0,1:T(2,128)(2,1)S(1)}, bf16[12,2]{0,1:T(2,128)(2,1)}, u32[]{:S(2)}) copy-start(bf16[12,2]{0,1:T(2,128)(2,1)} %param.38) | copy-start | bytes 148
  0.7 11.4 %copy-start.12 = (s32[12,2]{0,1:T(2,128)S(1)}, s32[12,2]{0,1:T(2,128)}, u32[]{:S(2)}) copy-start(s32[12,2]{0,1:T(2,128)} %param.37) | copy-start | bytes 292
  4.7 32.6 %copy-start.5 = (bf16[2048,64]{0,1:T(8,128)(2,1)S(1)}, bf16[2048,64]{0,1:T(8,128)(2,1)}, u32[]{:S(2)}) copy-start(bf16[2048,64]{0,1:T(8,128)(2,1)} %param.25) | copy-start | bytes 786436
  4.7 31.3 %all-to-all-start = ((bf16[16,12,2048]{2,1,0:T(8,128)(2,1)}), bf16[16,12,2048]{2,1,0:T(8,128)(2,1)}, u32[]{:S(2)}, u32[]{:S(2)}) async-start(bf16[16,12,2048]{2,1,0:T(8,128)(2,1)} %stack.12), calls=%async_computation | async-start | bytes 2097152 | tf_op jit(solution)/shard_map/all_to_all | solution.py:83
  11.3 26.4 %copy-start.6 = (bf16[2048,64]{0,1:T(8,128)(2,1)S(1)}, bf16[2048,64]{0,1:T(8,128)(2,1)}, u32[]{:S(2)}) copy-start(bf16[2048,64]{0,1:T(8,128)(2,1)} %param.26) | copy-start | bytes 786436
  11.7 26.4 %copy-start.11 = (f32[12,8]{0,1:T(8,128)}, f32[12,8]{0,1:T(8,128)S(1)}, u32[]{:S(2)}) copy-start(f32[12,8]{0,1:T(8,128)S(1)} %get-tuple-element.10) | copy-start | bytes 1156
  37.3 1.0 copy-start.7
  37.3 1.3 copy-start.8
  38.3 12.4 %copy-start.9 = (f32[12,8,128]{2,1,0:T(8,128)S(1)}, f32[12,8,128]{2,1,0:T(8,128)}, u32[]{:S(2)}) copy-start(f32[12,8,128]{2,1,0:T(8,128)} %param.34) | copy-start | bytes 147460
  40.1 9.9 %all-to-all-start.1 = ((bf16[16,2,1536]{2,1,0:T(2,128)(2,1)}), bf16[16,2,1536]{2,1,0:T(2,128)(2,1)S(1)}, u32[]{:S(2)}, u32[]{:S(2)}) async-start(bf16[16,2,1536]{2,1,0:T(2,128)(2,1)} %reshape.155), calls=%async_computation.1 | async-start | bytes 196608 | tf_op jit(solution)/shard_map/all_to_all | solution.py:100
  55.9 5.0 %copy-start.1 = (f32[12,8,128,128]{3,2,1,0:T(8,128)}, f32[12,8,128,128]{3,2,1,0:T(8,128)S(1)}, u32[]{:S(2)}) copy-start(f32[12,8,128,128]{3,2,1,0:T(8,128)S(1)} %multiply_add_fusion) | copy-start | bytes 18874372
  55.9 5.1 %copy-start.2 = (bf16[1024,2048]{1,0:T(8,128)(2,1)S(1)}, bf16[1024,2048]{1,0:T(8,128)(2,1)}, u32[]{:S(2)}) copy-start(bf16[1024,2048]{1,0:T(8,128)(2,1)} %param.36) | copy-start | bytes 12582916
  61.1 0.8 copy-start.3
  89.9 11.8 %all-to-all-start.2 = ((bf16[16,2,2048]{2,1,0:T(2,128)(2,1)}), bf16[16,2,2048]{2,1,0:T(2,128)(2,1)S(1)}, u32[]{:S(2)}, u32[]{:S(2)}) async-start(bf16[16,2,2048]{2,1,0:T(2,128)(2,1)} %copy.88), calls=%async_computation.2 | async-start | bytes 262144 | tf_op jit(solution)/shard_map/all_to_all | solution.py:45
  103.8 12.1 %copy-start.4 = (bf16[192,2048]{1,0:T(8,128)(2,1)S(1)}, bf16[192,2048]{1,0:T(8,128)(2,1)}, u32[]{:S(2)}) copy-start(bf16[192,2048]{1,0:T(8,128)(2,1)} %fusion.2) | copy-start | bytes 2359300
  107.0 54.9 %copy-start.13 = (u32[32]{0:T(128)S(1)}, u32[32]{0:T(128)}, u32[]{:S(2)}) copy-start(u32[32]{0:T(128)} %constant.42) | copy-start | bytes 388
  109.8 55.8 %all-to-all-start.3 = ((bf16[16,2,2048]{2,1,0:T(2,128)(2,1)}), bf16[16,2,2048]{2,1,0:T(2,128)(2,1)S(1)}, u32[]{:S(2)}, u32[]{:S(2)}) async-start(bf16[16,2,2048]{2,1,0:T(2,128)(2,1)} %reshape.157), calls=%async_computation.3 | async-start | bytes 262144 | tf_op jit(solution)/shard_map/all_to_all | solution.py:47
  144.5 20.4 %collective-permute-start = (bf16[16,2048]{1,0:T(8,128)(2,1)S(1)}, bf16[16,2048]{1,0:T(8,128)(2,1)S(1)}, u32[]{:S(2)}, u32[]{:S(2)}) collective-permute-start(bf16[16,2048]{1,0:T(8,128)(2,1)S(1)} %fusion), channel_id=1, source_target_pairs={{0,1},{1,2},{2,3},{3,4},{4,5},{5,6},{6,7},{7,8},{8,9},{9,10},{10,1... | collective-permute-start | bytes 196616
  147.2 17.7 %collective-permute-start.1 = (bf16[16,2048]{1,0:T(8,128)(2,1)S(1)}, bf16[16,2048]{1,0:T(8,128)(2,1)S(1)}, u32[]{:S(2)}, u32[]{:S(2)}) collective-permute-start(bf16[16,2048]{1,0:T(8,128)(2,1)S(1)} %fusion), channel_id=1, source_target_pairs={{0,2},{1,3},{2,4},{3,5},{4,6},{5,7},{6,8},{7,9},{8,10},{9,11},{10,... | collective-permute-start | bytes 196616
  152.6 12.3 %collective-permute-start.2 = (bf16[16,2048]{1,0:T(8,128)(2,1)S(1)}, bf16[16,2048]{1,0:T(8,128)(2,1)S(1)}, u32[]{:S(2)}, u32[]{:S(2)}) collective-permute-start(bf16[16,2048]{1,0:T(8,128)(2,1)S(1)} %fusion), channel_id=1, source_target_pairs={{0,3},{1,4},{2,5},{3,6},{4,7},{5,8},{6,9},{7,10},{8,11},{9,12},{10... | collective-permute-start | bytes 196616
  159.9 5.0 %collective-permute-start.3 = (bf16[12,2048]{1,0:T(8,128)(2,1)S(1)}, bf16[12,2048]{1,0:T(8,128)(2,1)S(1)}, u32[]{:S(2)}, u32[]{:S(2)}) collective-permute-start(bf16[12,2048]{1,0:T(8,128)(2,1)S(1)} %slice.36), channel_id=1, source_target_pairs={{0,4},{1,5},{2,6},{3,7},{4,8},{5,9},{6,10},{7,11},{8,12},{9,13},{1... | collective-permute-start | bytes 147464
